TPU v7x, 32 devices: a whole 2x2x4 slice. The times are simulated.
32 devices in a mesh: sp: 16 (over z, y, x), tp: 2 (over core).
Axes of the slice: x: 2, y: 2, z: 4, core: 2. Of those that a mesh axis runs over, the one named last changes fastest.
Arguments:
- tokens: bfloat16 [2048, 2048], P('sp', 'tp'), may hold values from -6 to 6
- in_gain: bfloat16 [1, 2048], P(None, 'tp'), may hold values from 0.099609375 to 1.8984375
- w_input: bfloat16 [2048, 1024], P(None, 'tp'), may hold values from -0.125 to 0.125
- w_bgate: bfloat16 [2048, 1024], P(None, 'tp'), may hold values from -0.125 to 0.125
- w_cgate: bfloat16 [2048, 1024], P(None, 'tp'), may hold values from -0.125 to 0.125
- w_value: bfloat16 [2048, 1024], P(None, 'tp'), may hold values from -0.125 to 0.125
- decay_rate: float32 [64, 64], P('tp'), may hold values from 9.765625e-05 to 0.034, as said below
- angle: float32 [64, 64], P('tp'), may hold values from -3.140625 to 3.140625
- decay_shift: float32 [64, 2048], P('tp', 'sp'), may hold values from -1.1 to 0, as said below
- b_input: float32 [2, 64, 64, 16], P(None, 'tp'), may hold values from -1 to 1
- c_output: float32 [2, 64, 16, 64], P(None, 'tp'), may hold values from -0.75 to 0.75
- initial_recurrence_vector: float32 [2, 64, 64], P(None, 'tp'), may hold values from -271.529 to 271.529
- skip_gain: float32 [1024], P('tp'), may hold values from -4 to 4
- ssm_gain: float32 [1024], P('tp'), may hold values from 0.1 to 1.9
- conv_gain: float32 [1024], P('tp'), may hold values from 0.1 to 1.9
- conv_taps: float32 [3, 1024], P(None, 'tp'), may hold values from -3.5 to 3.5
- w_out_ssm: bfloat16 [1024, 2048], P('tp'), may hold values from -0.125 to 0.125
- w_out_conv: bfloat16 [1024, 2048], P('tp'), may hold values from -0.125 to 0.125
Outputs:
- mixed: bfloat16 [2048, 2048], P(('sp', 'tp'))
Inputs may be any that keep to these rules, and one draw needn't show every extreme that they name: `decay_rate`: positive rates. `decay_shift`: never positive.
All inputs are finite; a program needn't handle non-finite values.
Results may differ from a plain program's by a relative error of at most 0.0085.
Values may be sent and summed in bfloat16 or wider, within the bound.
A program may use at most 64 MiB of HBM per device.

v0:
```python
import math

import jax
import jax.numpy as jnp
from jax import lax
from jax.sharding import PartitionSpec as P

D = 2048
GROUP_CH = 16
CONVOLUTION_CHAN = 64
KERNEL = 3


def entering(value, axis, join, neutral):
    count, mine = (lax.axis_size(axis), lax.axis_index(axis))
    pieces = jax.tree.map(lambda part: lax.all_gather(part, axis), value)
    subtotal = jax.tree.map(
        lambda part, zero: jnp.full_like(part, 0) + jnp.asarray(zero, part.dtype), value, neutral
    )

    def hop(position, subtotal):
        longer = join(subtotal, jax.tree.map(lambda part: part[position], pieces))
        return jax.tree.map(lambda new, old: jnp.where(position < mine, new, old), longer, subtotal)

    return lax.fori_loop(0, count - 1, hop, subtotal)


def from_behind(value, axis, steps):
    count = lax.axis_size(axis)
    initial, last = (max(0, -steps), min(count, count - steps))
    return lax.ppermute(value, axis, [(source, source + steps) for source in range(initial, last)])


def complex_step(first, second):
    ar1, ai1, br1, bi1 = first
    ar2, ai2, br2, bi2 = second
    return (
        ar2 * ar1 - ai2 * ai1,
        ar2 * ai1 + ai2 * ar1,
        ar2 * br1 - ai2 * bi1 + br2,
        ar2 * bi1 + ai2 * br1 + bi2,
    )


def input_matrix(decay_rate, angle, b_input):
    real_part = jnp.expm1(-decay_rate) * jnp.cos(angle) - 2.0 * jnp.sin(0.5 * angle) ** 2
    imag_part = jnp.exp(-decay_rate) * jnp.sin(angle)
    denom = decay_rate * decay_rate + angle * angle
    zoh_re = (imag_part * angle - real_part * decay_rate) / denom
    zoh_im = -(imag_part * decay_rate + real_part * angle) / denom
    b_re = zoh_re[..., None] * b_input[0] - zoh_im[..., None] * b_input[1]
    b_im = zoh_re[..., None] * b_input[1] + zoh_im[..., None] * b_input[0]
    return (b_re, b_im)


def head_norm(values, gain, width):
    count, total = values.shape
    grouped = values.reshape(count, total // width, width)
    grouped = grouped * lax.rsqrt(jnp.mean(grouped * grouped, axis=-1, keepdims=True) + 1e-06)
    return (grouped.reshape(count, total) * gain).astype(jnp.bfloat16)


def local_chain(drive_re, drive_im, shift_rows, rate_flat, theta_flat, entries):
    highest = lax.Precision.HIGHEST
    length, width = drive_re.shape
    blk = math.gcd(length, 128)
    rows_idx = lax.broadcasted_iota(jnp.int32, (blk, blk), 0)
    cols_idx = lax.broadcasted_iota(jnp.int32, (blk, blk), 1)
    lower = (rows_idx >= cols_idx).astype(jnp.float32)
    counted = (lax.broadcasted_iota(jnp.int32, (blk, 1), 0) + 1).astype(jnp.float32)
    carry_pr = jnp.ones((1, width), jnp.float32)
    carry_pi = jnp.zeros((1, width), jnp.float32)
    carry_sr = jnp.zeros((1, width), jnp.float32)
    carry_si = jnp.zeros((1, width), jnp.float32)
    pieces = ([], [], [], [])
    local_log = jnp.dot(lower, shift_rows, precision=highest)
    log_mag = jnp.repeat(local_log, entries, axis=1) - counted * rate_flat
    phase = counted * theta_flat
    cosine = jnp.cos(phase)
    sine = jnp.sin(phase)
    magnitude = jnp.exp(log_mag)
    inverse = jnp.exp(-log_mag)
    quot_re = inverse * (drive_re * cosine + drive_im * sine)
    quot_im = inverse * (drive_im * cosine - drive_re * sine)
    summed_re = jnp.dot(lower, quot_re, precision=highest)
    summed_im = jnp.dot(lower, quot_im, precision=highest)
    prod_re = magnitude * cosine
    prod_im = magnitude * sine
    inner_re = prod_re * summed_re - prod_im * summed_im
    inner_im = prod_re * summed_im + prod_im * summed_re
    cum_re = prod_re * carry_pr - prod_im * carry_pi
    cum_im = prod_re * carry_pi + prod_im * carry_pr
    st_re = inner_re + prod_re * carry_sr - prod_im * carry_si
    st_im = inner_im + prod_re * carry_si + prod_im * carry_sr
    pieces[0].append(cum_re)
    pieces[1].append(cum_im)
    pieces[2].append(st_re)
    pieces[3].append(st_im)
    return tuple((items[0] for items in pieces))


def body(
    tokens,
    in_gain,
    w_input,
    w_bgate,
    w_cgate,
    w_value,
    decay_rate,
    angle,
    decay_shift,
    b_input,
    c_output,
    initial_recurrence_vector,
    skip_gain,
    ssm_gain,
    conv_gain,
    conv_taps,
    w_out_ssm,
    w_out_conv,
):
    highest = lax.Precision.HIGHEST
    length = tokens.shape[0]
    ssm_width = w_input.shape[1]
    filter_tap_length = w_bgate.shape[1]
    merged_result = jnp.concatenate([w_input, w_bgate, w_cgate, w_value], axis=1)
    piece = lax.all_gather(tokens, "tp", axis=1, tiled=True)
    gain = lax.all_gather(in_gain, "tp", axis=1, tiled=True)
    floats = piece.astype(jnp.float32)
    scaled = (floats * gain.astype(jnp.float32)).astype(jnp.bfloat16)
    accum = jnp.dot(scaled, merged_result, preferred_element_type=jnp.float32)
    accum, squares = (accum, jnp.sum(floats * floats, axis=1))
    inv = lax.rsqrt(squares / D + 1e-06)
    projected = (accum * inv[:, None]).astype(jnp.bfloat16)
    u_in = projected[:, 0:ssm_width]
    bgate = projected[:, ssm_width : ssm_width + filter_tap_length]
    cgate = projected[:, ssm_width + filter_tap_length : ssm_width + 2 * filter_tap_length]
    value = projected[:, ssm_width + 2 * filter_tap_length : ssm_width + 3 * filter_tap_length]
    groups = decay_rate.shape[0]
    entries = decay_rate.shape[1]
    width = groups * entries
    b_re, b_im = input_matrix(decay_rate, angle, b_input)
    u_float = u_in.astype(jnp.float32)
    u_groups = u_float.reshape(length, groups, GROUP_CH)
    drive_re = jnp.einsum("lgh,gph->lgp", u_groups, b_re, precision=highest).reshape(length, width)
    drive_im = jnp.einsum("lgh,gph->lgp", u_groups, b_im, precision=highest).reshape(length, width)
    cum = local_chain(
        drive_re,
        drive_im,
        decay_shift.T,
        decay_rate.reshape(1, width),
        angle.reshape(1, width),
        entries,
    )
    totals = tuple((item[length - 1].reshape(groups, entries) for item in cum))
    ones = jnp.ones((groups, entries), jnp.float32)
    zeros = jnp.zeros((groups, entries), jnp.float32)
    gated = cgate.astype(jnp.float32) * value.astype(jnp.float32)
    tail = gated[length - (KERNEL - 1) :]
    before = entering(totals, "sp", complex_step, (ones, zeros, zeros, zeros))
    prior = from_behind(tail, "sp", 1)
    entry_re = (
        before[0] * initial_recurrence_vector[0]
        - before[1] * initial_recurrence_vector[1]
        + before[2]
    )
    entry_im = (
        before[0] * initial_recurrence_vector[1]
        + before[1] * initial_recurrence_vector[0]
        + before[3]
    )
    entry_re = entry_re.reshape(1, width)
    entry_im = entry_im.reshape(1, width)
    state_re = (cum[2] + cum[0] * entry_re - cum[1] * entry_im).reshape(length, groups, entries)
    state_im = (cum[3] + cum[0] * entry_im + cum[1] * entry_re).reshape(length, groups, entries)
    read_out = jnp.einsum("lgp,ghp->lgh", state_re, c_output[0], precision=highest)
    read_out = read_out - jnp.einsum("lgp,ghp->lgh", state_im, c_output[1], precision=highest)
    ssm_pre = read_out.reshape(length, ssm_width) + skip_gain * u_float
    state_space_output = head_norm(jax.nn.gelu(ssm_pre, approximate=False), ssm_gain, GROUP_CH)
    padded = jnp.concatenate([prior, gated], axis=0)
    conv = padded[0:length] * conv_taps[0]
    for tap in range(1, KERNEL):
        conv = conv + padded[tap : tap + length] * conv_taps[tap]
    conv_out = head_norm(bgate.astype(jnp.float32) * conv, conv_gain, CONVOLUTION_CHAN)
    result = jnp.dot(state_space_output, w_out_ssm, preferred_element_type=jnp.float32)
    return lax.psum_scatter(
        (result + jnp.dot(conv_out, w_out_conv, preferred_element_type=jnp.float32)).astype(
            jnp.bfloat16
        ),
        "tp",
        scatter_dimension=0,
        tiled=True,
    )


def solution(mesh):
    return jax.shard_map(
        body,
        mesh=mesh,
        in_specs=(
            P("sp", "tp"),
            P(None, "tp"),
            P(None, "tp"),
            P(None, "tp"),
            P(None, "tp"),
            P(None, "tp"),
            P("tp", None),
            P("tp", None),
            P("tp", "sp"),
            P(None, "tp", None, None),
            P(None, "tp", None, None),
            P(None, "tp", None),
            P("tp"),
            P("tp"),
            P("tp"),
            P(None, "tp"),
            P("tp", None),
            P("tp", None),
        ),
        out_specs=P(("sp", "tp"), None),
        check_vma=False,
    )
```

profile of v0, /device:TPU:0, one launch (start us, length us, event | category | flops | bytes accessed | tf_op | source)
XLA Modules:
  0.0 261.3 jit_solution(6176383883041649938)
XLA Ops:
  6.5 2.6 %all_gather.18 = bf16[128,2048]{1,0:T(8,128)(2,1)S(1)} all-gather(bf16[128,1024]{1,0:T(8,128)(2,1)} %param.20), channel_id=1, replica_groups=mesh['sp'=16,'tp'=2] {'tp'}, dimensions={1}, use_global_device_ids=true | all-gather | bytes 786432 | tf_op jit(solution)/shard_map/all_gather | solution.py:127
  9.4 2.0 all_gather.19
  11.4 4.3 %fusion.19 = bf16[128,2048]{1,0:T(8,128)(2,1)S(1)} fusion(bf16[2048,512]{1,0:T(8,128)(2,1)} %param.25, bf16[2048,512]{1,0:T(8,128)(2,1)} %param.24, bf16[2048,512]{1,0:T(8,128)(2,1)} %param.23, bf16[2048,512]{1,0:T(8,128)(2,1)} %param.22, bf16[128,2048]{1,0:T(8,128)(2,1)S(1)} %all_gather.18, f32[128]{0:T(128)S(1)} %add_rsqrt_fusion.2, f32[2048]{0:T(1024)S(1)} %bitcast.133), kind=kOutput, calls=%fused_computation.28 | convolution fusion | flops 1108606976 | bytes 9445888 | tf_op jit(solution)/shard_map/dot_general | solution.py:131
  15.8 4.7 %collective-permute-start = (f32[2,512]{1,0:T(2,128)S(1)}, f32[2,512]{1,0:T(2,128)S(1)}, u32[]{:S(2)}, u32[]{:S(2)}) collective-permute-start(f32[2,512]{1,0:T(2,128)S(1)} %slice.92), channel_id=1, source_target_pairs={{0,2},{2,4},{4,6},{6,8},{8,10},{10,12},{12,14},{14,16},{16,18},{18... | collective-permute-start | bytes 12296 | tf_op jit(solution)/shard_map/ppermute | solution.py:31
  20.9 2.0 fusion.61
  22.9 2.0 fusion.64
  25.0 1.6 copy.44
  26.6 2.5 copy.45
  30.4 2.6 copy.42
  33.0 6.3 %fusion.37 = f32[128,2048]{1,0:T(8,128)S(1)} fusion(f32[128,2048]{1,0:T(8,128)S(1)} %copy.44, f32[128,2048]{1,0:T(8,128)} %copy.45, f32[128,2048]{1,0:T(8,128)} %copy.42, f32[2048]{0:T(1024)S(1)} %mul.377, f32[2048]{0:T(1024)S(1)} %mul.374, f32[128]{0:T(128)S(1)} %add_convert_fusion), kind=kOutput, calls=%fused_computation.48 | convolution fusion | flops 404766720 | bytes 4211200 | tf_op jit(solution)/shard_map/dot_general | solution.py:86
  39.3 10.2 %add_add_fusion = (f32[128,2048]{1,0:T(8,128)}, f32[128,2048]{1,0:T(8,128)}, f32[128,2048]{1,0:T(8,128)}, f32[128,2048]{1,0:T(8,128)S(1)}) fusion(f32[128,2048]{1,0:T(8,128)S(1)} %fusion.37, f32[2048]{0:T(1024)S(1)} %mul.377, f32[128,2048]{1,0:T(8,128)S(1)} %copy-done.2, f32[2048]{0:T(1024)S(1)} %mul.374, f32[128]{0:T(128)S(1)} %add_convert_fusion, ...), kind=kOutput, calls=%fused_computation.51 | convolution fusion | flops 409747456 | bytes 8405504 | tf_op jit(solution)/shard_map/dot_general | solution.py:85
  50.6 42.7 %all_gather.20 = f32[16,32,64]{2,1,0:T(8,128)} all-gather(f32[1,32,64]{2,1,0:T(8,128)S(1)} %all_gather_reshape_squeeze.12), channel_id=1, replica_groups=mesh['sp'=16,'tp'=2] {'sp'}, dimensions={0}, use_global_device_ids=true | all-gather | bytes 139264 | tf_op jit(solution)/shard_map/all_gather | solution.py:16
  94.3 39.2 %all_gather.21 = f32[16,32,64]{2,1,0:T(8,128)} all-gather(f32[1,32,64]{2,1,0:T(8,128)S(1)} %all_gather_reshape_squeeze.13), channel_id=1, replica_groups=mesh['sp'=16,'tp'=2] {'sp'}, dimensions={0}, use_global_device_ids=true | all-gather | bytes 139264 | tf_op jit(solution)/shard_map/all_gather | solution.py:16
  134.4 41.3 %all_gather.22 = f32[16,32,64]{2,1,0:T(8,128)} all-gather(f32[1,32,64]{2,1,0:T(8,128)S(1)} %all_gather_reshape_squeeze.14), channel_id=1, replica_groups=mesh['sp'=16,'tp'=2] {'sp'}, dimensions={0}, use_global_device_ids=true | all-gather | bytes 139264 | tf_op jit(solution)/shard_map/all_gather | solution.py:16
  176.7 39.4 %all_gather.23 = f32[16,32,64]{2,1,0:T(8,128)} all-gather(f32[1,32,64]{2,1,0:T(8,128)S(1)} %all_gather_reshape_squeeze.15), channel_id=1, replica_groups=mesh['sp'=16,'tp'=2] {'sp'}, dimensions={0}, use_global_device_ids=true | all-gather | bytes 139264 | tf_op jit(solution)/shard_map/all_gather | solution.py:16
  216.1 12.3 %while.20 = (s32[]{:T(128)}, f32[32,64]{1,0:T(8,128)S(1)}, f32[32,64]{1,0:T(8,128)S(1)}, f32[32,64]{1,0:T(8,128)S(1)}, f32[32,64]{1,0:T(8,128)S(1)}, /*index=5*/...) while((s32[]{:T(128)}, f32[32,64]{1,0:T(8,128)S(1)}, ...), condition=%wide.region_2.3_spmd.clone, body=%wide.region_1.2_spmd.clone.sunk | while | flops 45060 | bytes 98445 | solution.py:25
  228.5 3.7 %multiply_add_fusion = (f32[128,2048]{1,0:T(8,128)}, f32[128,2048]{1,0:T(8,128)}) fusion(f32[128,2048]{1,0:T(8,128)} %get-tuple-element.246, f32[128,2048]{1,0:T(8,128)S(1)} %copy-done.3, f32[128,2048]{1,0:T(8,128)} %copy-done.4, f32[2048]{0:T(1024)S(1)} %mul.426, f32[2048]{0:T(1024)S(1)} %mul.421, f32[128,2048]{1,0:T(8,128)} %get-tuple-element.243), kind=kLoop, calls=%fused_computation.49 | loop fusion | flops 2097152 | bytes 6307840 | tf_op jit(solution)/shard_map/add | solution.py:175
  232.2 2.5 copy.48
  234.7 1.5 copy.49
  236.3 2.3 fusion.58
  238.6 2.7 %convolution_subtract_fusion = f32[32,128,16]{1,2,0:T(8,128)} fusion(f32[32,128,16]{1,2,0:T(8,128)S(1)} %fusion.58, f32[128,32,64]{0,2,1:T(8,128)S(1)} %bitcast.120, f32[2,32,16,64]{3,2,1,0:T(8,128)} %param.30), kind=kOutput, calls=%fused_computation.40 | convolution fusion | flops 50397184 | bytes 1835008 | tf_op jit(solution)/shard_map/lgp,ghp->lgh/dot_general | solution.py:177
  242.4 2.3 fusion.95
  245.5 2.1 fusion.79
  248.9 5.6 %reduce-scatter.2.cloned.1.call-done = bf16[64,2048]{1,0:T(8,128)(2,1)} async-done(((bf16[128,2048]{1,0:T(8,128)(2,1)}), bf16[64,2048]{1,0:T(8,128)(2,1)}) %reduce-scatter.2.cloned.1.call-update) | async-done | bytes 262160 | tf_op jit(solution)/shard_map/reduce_scatter | solution.py:186
  (93 shorter events, 20.9 us)
Async XLA Ops:
  6.5 238.9 %copy-start = (bf16[512,2048]{1,0:T(8,128)(2,1)S(1)}, bf16[512,2048]{1,0:T(8,128)(2,1)}, u32[]{:S(2)}) copy-start(bf16[512,2048]{1,0:T(8,128)(2,1)} %param.36) | copy-start | bytes 6291460
  6.5 248.0 %reduce-scatter.2.cloned.1.call-start = ((), (), s32[]{:S(2)}) async-start(), calls=%async_computation.1 | async-start | bytes 786432 | tf_op jit(solution)/shard_map/reduce_scatter | solution.py:186
  11.4 9.3 %copy-start.9 = (f32[32,64]{1,0:T(8,128)S(1)}, f32[32,64]{1,0:T(8,128)}, u32[]{:S(2)}) copy-start(f32[32,64]{1,0:T(8,128)} %param.26) | copy-start | bytes 24580
  11.4 9.3 %copy-start.10 = (f32[32,64]{1,0:T(8,128)S(1)}, f32[32,64]{1,0:T(8,128)}, u32[]{:S(2)}) copy-start(f32[32,64]{1,0:T(8,128)} %param.27) | copy-start | bytes 24580
  11.4 9.5 %copy-start.8 = (f32[2,32,64,16]{2,3,1,0:T(8,128)S(1)}, f32[2,32,64,16]{2,3,1,0:T(8,128)}, u32[]{:S(2)}) copy-start(f32[2,32,64,16]{2,3,1,0:T(8,128)} %param.29) | copy-start | bytes 786436
  15.7 4.8 %copy-start.7 = (bf16[128,2048]{1,0:T(8,128)(2,1)}, bf16[128,2048]{1,0:T(8,128)(2,1)S(1)}, u32[]{:S(2)}) copy-start(bf16[128,2048]{1,0:T(8,128)(2,1)S(1)} %fusion.19) | copy-start | bytes 1572868
  15.8 226.6 %collective-permute-start = (f32[2,512]{1,0:T(2,128)S(1)}, f32[2,512]{1,0:T(2,128)S(1)}, u32[]{:S(2)}, u32[]{:S(2)}) collective-permute-start(f32[2,512]{1,0:T(2,128)S(1)} %slice.92), channel_id=1, source_target_pairs={{0,2},{2,4},{4,6},{6,8},{8,10},{10,12},{12,14},{14,16},{16,18},{18... | collective-permute-start | bytes 12296 | tf_op jit(solution)/shard_map/ppermute | solution.py:31
  25.0 4.1 %copy-start.12 = (f32[32,128]{1,0:T(8,128)S(1)}, f32[32,128]{1,0:T(8,128)}, u32[]{:S(2)}) copy-start(f32[32,128]{1,0:T(8,128)} %param.28) | copy-start | bytes 49156
  33.0 6.3 %copy-start.1 = (f32[128,2048]{1,0:T(8,128)S(1)}, f32[128,2048]{1,0:T(8,128)}, u32[]{:S(2)}) copy-start(f32[128,2048]{1,0:T(8,128)} %copy.45) | copy-start | bytes 3145732
  33.0 6.3 %copy-start.2 = (f32[128,2048]{1,0:T(8,128)S(1)}, f32[128,2048]{1,0:T(8,128)}, u32[]{:S(2)}) copy-start(f32[128,2048]{1,0:T(8,128)} %copy.42) | copy-start | bytes 3145732
  49.5 1.0 copy-start.4
  49.5 178.8 %copy-start.11 = (f32[2,32,64]{2,1,0:T(8,128)S(1)}, f32[2,32,64]{2,1,0:T(8,128)}, u32[]{:S(2)}) copy-start(f32[2,32,64]{2,1,0:T(8,128)} %param.31) | copy-start | bytes 49156
  49.5 179.0 %copy-start.3 = (f32[128,2048]{1,0:T(8,128)S(1)}, f32[128,2048]{1,0:T(8,128)}, u32[]{:S(2)}) copy-start(f32[128,2048]{1,0:T(8,128)} %get-tuple-element.242) | copy-start | bytes 3145732
  236.3 5.0 %copy-start.13 = (f32[3,512]{1,0:T(4,128)S(1)}, f32[3,512]{1,0:T(4,128)}, u32[]{:S(2)}) copy-start(f32[3,512]{1,0:T(4,128)} %param.35) | copy-start | bytes 18436
  236.3 6.1 %copy-start.14 = (f32[512]{0:T(512)S(1)}, f32[512]{0:T(512)}, u32[]{:S(2)}) copy-start(f32[512]{0:T(512)} %param.32) | copy-start | bytes 6148
  242.4 3.1 %copy-start.16 = (f32[512]{0:T(512)S(1)}, f32[512]{0:T(512)}, u32[]{:S(2)}) copy-start(f32[512]{0:T(512)} %param.33) | copy-start | bytes 6148
  245.5 2.1 copy-start.5
  245.5 2.1 copy-start.6
  245.5 2.1 copy-start.15
Sparse Core Ops, SparseCore 0:
  249.0 5.4 reduce-scatter.1
where the time goes:
time: 264 us; the launch traced here: 261 us
  blocking collectives  167 us (63%)
  matrix products  33.2 us (13%)
  other arithmetic  18.4 us (7%)
  local copies, waits for them, and re-layouts  17.9 us (7%)
  between operations  13.8 us (5%)
  waiting for transfers between devices  5.66 us (2%)
  starting transfers between devices  4.73 us (2%)
    all_gather x4, blocking collectives, entering(): pieces = jax.tree.map(lambda part: lax.all_gather(part, axis), value)  163 us
    select_n x15, other arithmetic, hop(): jnp.where(position < mine, new, old)  11.9 us
    dot_general x1, matrix products, local_chain(): summed_re = jnp.dot(lower, quot_re, precision=highest)  10.2 us
    dot_general x1, matrix products, local_chain(): summed_im = jnp.dot(lower, quot_im, precision=highest)  6.28 us
    reduce_scatter x1, waiting for transfers between devices, body(): lax.psum_scatter((result + jnp.dot(conv_out, w_out_conv, preferred_elemen...  5.64 us
  transfers between devices with their start and end apart: 2, of which 1 were waited for; matrix products, arithmetic and copies ran while one was open for 22% of the time, Pallas kernels for 0%

commit v1 on v0

v1 whole, which is shorter than its diff:
```python
import functools

import jax
import jax.numpy as jnp
from jax import lax
from jax.experimental import pallas as pl
from jax.experimental.pallas import tpu as pltpu
from jax.sharding import PartitionSpec as P

CONVOLUTION_CHAN = 64
KERNEL = 3
MESH = pl.DeviceIdType.MESH
F32 = jnp.float32
BF16 = jnp.bfloat16


def inner_size(count):
    size = 1
    while size * size < count:
        size *= 2
    return size


def dot(a, b):
    return jnp.dot(a, b, preferred_element_type=F32)


def dot_nt(a, b):
    return lax.dot_general(a, b, (((1,), (1,)), ((), ())), preferred_element_type=F32)


def expm1_of(x):
    series = x * (1 + x / 2 * (1 + x / 3 * (1 + x / 4 * (1 + x / 5 * (1 + x / 6)))))
    return jnp.where(jnp.abs(x) < 0.125, series, jnp.exp(x) - 1)


def zoh_of(rate, angle):
    real_part = expm1_of(-rate) * jnp.cos(angle) - 2.0 * jnp.sin(0.5 * angle) ** 2
    imag_part = jnp.exp(-rate) * jnp.sin(angle)
    denom = rate * rate + angle * angle
    return (
        (imag_part * angle - real_part * rate) / denom,
        -(imag_part * rate + real_part * angle) / denom,
    )


def split3(x):
    hi = x.astype(BF16).astype(F32)
    mid = (x - hi).astype(BF16).astype(F32)
    return hi, mid, x - hi - mid


def kernel(
    sizes,
    tok_h, gain, w_in_h, w_bg_h, w_cg_h, w_va_h, rate, angle, shift, b_in, c_out, init,
    skip, sgain, cgain, taps, wos_h, woc_h,
    out,
    tok, gain_o, w, wos, woc, sc, bx, cx, e_s, d_re, d_im, gated, halo, acc, ssm_b,
    mine1, slots1, mine2, slots2, part_s, part_r,
    loc_sem, tok_send, tok_recv, ph1_send, ph1_recv, ph2_send, ph2_recv, halo_send, halo_recv,
    out_send, out_recv,
):
    nsp, n1, n2 = sizes
    sp, tp = lax.axis_index("sp"), lax.axis_index("tp")
    rows, half = tok_h.shape
    groups, entries = rate.shape
    ch = c_out.shape[2]
    per = 128 // ch
    width = groups * entries
    lines = width // 128
    blocks = groups // per
    wide = per * entries
    inner, outer = lax.rem(sp, n1), lax.div(sp, n1)
    nxt, prv = lax.rem(sp + 1, nsp), lax.rem(sp + nsp - 1, nsp)

    def half_of(ref, which):
        start = (tp if which == 0 else 1 - tp) * half
        return ref.at[pl.ds(pl.multiple_of(start, half), half), :]

    copies = [pltpu.make_async_copy(tok_h, tok.at[0], loc_sem.at[0])]
    for number, ref in enumerate((w_in_h, w_cg_h, w_va_h, w_bg_h)):
        for which in range(2):
            copies.append(
                pltpu.make_async_copy(
                    half_of(ref, which), w.at[number, which], loc_sem.at[len(copies)]
                )
            )
    copies.append(pltpu.make_async_copy(woc_h, woc, loc_sem.at[len(copies)]))
    copies.append(pltpu.make_async_copy(wos_h, wos, loc_sem.at[len(copies)]))
    for copy in copies:
        copy.start()

    peers1 = [outer * n1 + lax.rem(inner + k, n1) for k in range(1, n1)]
    peers2 = [lax.rem(outer + k, n2) * n1 + inner for k in range(1, n2)]
    barrier = pltpu.get_barrier_semaphore()
    pl.semaphore_signal(barrier, inc=1, device_id={"tp": 1 - tp}, device_id_type=MESH)
    for peer in peers1 + peers2 + [nxt, prv]:
        pl.semaphore_signal(barrier, inc=1, device_id={"sp": peer}, device_id_type=MESH)
    pl.semaphore_wait(barrier, 1 + len(peers1) + len(peers2) + 2)

    def remote(src, dst, send, recv, **where):
        return pltpu.make_async_remote_copy(
            src_ref=src, dst_ref=dst, send_sem=send, recv_sem=recv,
            device_id=where, device_id_type=MESH,
        )

    swap_tok = remote(tok_h, tok.at[1], tok_send.at[0], tok_recv.at[0], tp=1 - tp)
    swap_gain = remote(gain, gain_o, tok_send.at[1], tok_recv.at[1], tp=1 - tp)
    swap_tok.start()
    swap_gain.start()

    bx[...] = jnp.zeros_like(bx)
    cx[...] = jnp.zeros_like(cx)
    zr, zi = zoh_of(rate[...], angle[...])
    for g in range(groups):
        q, k = g // per, g % per
        r, l = k * ch, k * entries
        gr, gi = zr[g : g + 1, :], zi[g : g + 1, :]
        b0, b1 = b_in[0, g], b_in[1, g]
        bx[q, r : r + ch, l : l + entries] = (gr * b0 - gi * b1).astype(BF16)
        bx[q, r : r + ch, wide + l : wide + l + entries] = (gr * b1 + gi * b0).astype(BF16)
        cx[q, r : r + ch, l : l + entries] = c_out[0, g].astype(BF16)
        cx[q, r : r + ch, wide + l : wide + l + entries] = (-c_out[1, g]).astype(BF16)

    parts = jnp.concatenate(split3(jnp.exp(shift[...])), axis=0)
    count = parts.shape[0]
    pad = -count % 128
    if pad:
        parts = jnp.concatenate([parts, jnp.zeros((pad, rows), F32)], axis=0)
    parts = parts.T.astype(BF16)
    kk = lax.broadcasted_iota(jnp.int32, (count + pad, 128), 0)
    cc = lax.broadcasted_iota(jnp.int32, (count + pad, 128), 1)
    for j in range(lines):
        owner = (cc + j * 128) // entries
        spread = jnp.where((kk < count) & (lax.rem(kk, groups) == owner), 1.0, 0.0).astype(BF16)
        e_s[pl.ds(j, rows, stride=lines), :] = dot(parts, spread)

    def packed(ref):
        left = ref[pl.ds(0, lines, stride=2), :]
        right = ref[pl.ds(1, lines, stride=2), :]
        return jnp.concatenate([left, right], axis=1)

    rate_p, angle_p = packed(rate), packed(angle)
    size = jnp.exp(-rate_p)
    lam_re, lam_im = size * jnp.cos(angle_p), size * jnp.sin(angle_p)

    copies[0].wait()
    floats = tok[0].astype(F32)
    sc[0] = (floats * gain[...].astype(F32)).astype(BF16)
    squares = jnp.sum(floats * floats, axis=1, keepdims=True)
    copies[1].wait()
    total = dot(sc[0], w[0, 0])
    swap_tok.wait()
    swap_gain.wait()
    floats = tok[1].astype(F32)
    sc[1] = (floats * gain_o[...].astype(F32)).astype(BF16)
    squares = squares + jnp.sum(floats * floats, axis=1, keepdims=True)
    inv = lax.rsqrt(squares / (2 * half) + 1e-06)
    copies[2].wait()
    total = total + dot(sc[1], w[0, 1])
    u = (total * inv).astype(BF16)
    for q in range(blocks):
        drive = dot(u[:, q * 128 : (q + 1) * 128], bx[q])
        for k in range(wide // 128):
            j = q * (wide // 128) + k
            d_re[pl.ds(j, rows, stride=lines), :] = drive[:, k * 128 : (k + 1) * 128]
            d_im[pl.ds(j, rows, stride=lines), :] = drive[:, wide + k * 128 : wide + (k + 1) * 128]

    def advance(n, s_re, s_im):
        here = pl.ds(pl.multiple_of(n * lines, lines), lines)
        decay = e_s[here, :]
        a_re, a_im = lam_re * decay, lam_im * decay
        new_re = (a_re * s_re - a_im * s_im) + d_re[here, :]
        new_im = (a_re * s_im + a_im * s_re) + d_im[here, :]
        return here, decay, new_re, new_im

    unroll = 8
    nil = jnp.zeros((lines, 128), F32)

    def first_pass(t, carry):
        s_re, s_im, kept = carry
        for k in range(unroll):
            _, decay, s_re, s_im = advance(t * unroll + k, s_re, s_im)
            kept = kept * decay
        return s_re, s_im, kept

    s_re, s_im, kept = lax.fori_loop(0, rows // unroll, first_pass, (nil, nil, nil + 1.0))
    mine1[0] = s_re
    mine1[1] = s_im
    mine1[2] = kept
    slots1[0, 0] = s_re
    slots1[0, 1] = s_im
    slots1[0, 2] = kept
    sends1 = []
    for k, peer in enumerate(peers1, 1):
        sends1.append(
            remote(mine1, slots1.at[k], ph1_send.at[k], ph1_recv.at[k], sp=peer)
        )
        sends1[-1].start()

    def power(re, im, exponent):
        out_re, out_im = None, None
        while exponent:
            if exponent % 2:
                if out_re is None:
                    out_re, out_im = re, im
                else:
                    out_re, out_im = out_re * re - out_im * im, out_re * im + out_im * re
            re, im = re * re - im * im, 2.0 * re * im
            exponent //= 2
        return out_re, out_im

    lam1_re, lam1_im = power(lam_re, lam_im, rows)
    lam2_re, lam2_im = power(lam1_re, lam1_im, n1)

    def project(number):
        copies[1 + 2 * number].wait()
        value = dot(sc[0], w[number, 0])
        copies[2 + 2 * number].wait()
        value = value + dot(sc[1], w[number, 1])
        return (value * inv).astype(BF16).astype(F32)

    cg = project(1)
    gated[8:, :] = cg * project(2)
    swap_halo = remote(
        gated.at[pl.ds(rows, 8), :], halo, halo_send.at[0], halo_recv.at[0], sp=nxt
    )
    swap_halo.start()

    def follow(state, slot, p_re, p_im, use):
        re, im = state
        keep = slot[2]
        a_re, a_im = p_re * keep, p_im * keep
        new_re = a_re * re - a_im * im + slot[0]
        new_im = a_re * im + a_im * re + slot[1]
        if use is None:
            return new_re, new_im
        return jnp.where(use, new_re, re), jnp.where(use, new_im, im)

    for send in sends1:
        send.wait()
    state, kept = (nil, nil), nil + 1.0
    for member in range(n1):
        slot = slots1[lax.rem(inner - member + n1, n1)]
        state = follow(state, slot, lam1_re, lam1_im, None)
        kept = kept * slot[2]
    mine2[0], mine2[1], mine2[2] = state[0], state[1], kept
    slots2[0, 0], slots2[0, 1], slots2[0, 2] = state[0], state[1], kept
    sends2 = []
    for k, peer in enumerate(peers2, 1):
        sends2.append(
            remote(mine2, slots2.at[k], ph2_send.at[k], ph2_recv.at[k], sp=peer)
        )
        sends2[-1].start()

    bg = project(3)
    swap_halo.wait()
    gated[0:8, :] = jnp.where(sp > 0, halo[...], 0.0)
    conv = None
    for tap in range(KERNEL):
        lo = 8 - (KERNEL - 1) + tap
        term = gated[lo : lo + rows, :] * taps[tap : tap + 1, :]
        conv = term if conv is None else conv + term
    conv = bg * conv

    def head_norm(values, gains, head):
        r = lax.broadcasted_iota(jnp.int32, (128, 128), 0) // head
        c = lax.broadcasted_iota(jnp.int32, (128, 128), 1) // head
        mean = jnp.where(r == c, 1.0 / head, 0.0).astype(BF16)
        pieces = []
        for q in range(values.shape[1] // 128):
            v = values[:, q * 128 : (q + 1) * 128]
            scale = lax.rsqrt(dot((v * v).astype(BF16), mean) + 1e-06)
            pieces.append((v * scale * gains[:, q * 128 : (q + 1) * 128]).astype(BF16))
        return jnp.concatenate(pieces, axis=1)

    conv_b = head_norm(conv, cgain[...], CONVOLUTION_CHAN)
    copies[9].wait()
    acc[...] = dot(conv_b, woc[...])

    for send in sends2:
        send.wait()
    state = (packed(init.at[0]), packed(init.at[1]))
    for member in range(n2 - 1):
        slot = slots2[lax.rem(outer - member + n2, n2)]
        state = follow(state, slot, lam2_re, lam2_im, member < outer)
    for member in range(n1 - 1):
        slot = slots1[lax.rem(inner - member + n1, n1)]
        state = follow(state, slot, lam1_re, lam1_im, member < inner)

    def second_pass(t, carry):
        s_re, s_im = carry
        for k in range(unroll):
            here, _, s_re, s_im = advance(t * unroll + k, s_re, s_im)
            d_re[here, :] = s_re
            d_im[here, :] = s_im
        return s_re, s_im

    lax.fori_loop(0, rows // unroll, second_pass, state)
    for q in range(blocks):
        pieces = []
        for ref in (d_re, d_im):
            for k in range(wide // 128):
                j = q * (wide // 128) + k
                pieces.append(ref[pl.ds(j, rows, stride=lines), :].astype(BF16))
        y = dot_nt(jnp.concatenate(pieces, axis=1), cx[q])
        cols = slice(q * 128, (q + 1) * 128)
        pre = y + skip[:, cols] * u[:, cols].astype(F32)
        act = 0.5 * pre * (1.0 + lax.erf(pre * (0.5**0.5)))
        ssm_b[:, cols] = head_norm(act, sgain[:, cols], ch)

    copies[10].wait()
    total_cols = wos.shape[1]
    chunks = part_r.shape[0]
    step = total_cols // chunks
    part_rows = rows // 2
    own = pl.ds(pl.multiple_of(tp * part_rows, part_rows), part_rows)
    other = pl.ds(pl.multiple_of((1 - tp) * part_rows, part_rows), part_rows)
    sends = []
    for c in range(chunks):
        cols = slice(c * step, (c + 1) * step)
        part_s[c] = (acc[:, cols] + dot(ssm_b[...], wos[:, cols])).astype(BF16)
        sends.append(
            remote(part_s.at[c, other], part_r.at[c], out_send.at[c], out_recv.at[c], tp=1 - tp)
        )
        sends[-1].start()
    for c in range(chunks):
        sends[c].wait()
        cols = slice(c * step, (c + 1) * step)
        out[:, cols] = (part_s[c, own].astype(F32) + part_r[c].astype(F32)).astype(BF16)


def body(
    nsp,
    tokens, in_gain, w_input, w_bgate, w_cgate, w_value, decay_rate, angle, decay_shift,
    b_input, c_output, init, skip_gain, ssm_gain, conv_gain, conv_taps, w_out_ssm, w_out_conv,
):
    rows, half = tokens.shape
    groups, entries = decay_rate.shape
    lines = groups * entries // 128
    ch = c_output.shape[2]
    inner = w_input.shape[1]
    blocks = groups // (128 // ch)
    wide = (128 // ch) * entries
    n1 = inner_size(nsp)
    n2 = nsp // n1
    total_cols = w_out_ssm.shape[1]
    chunks = 4
    vmem = pl.BlockSpec(memory_space=pltpu.VMEM)
    hbm = pl.BlockSpec(memory_space=pl.ANY)
    dma = pltpu.SemaphoreType.DMA
    return pl.pallas_call(
        functools.partial(kernel, (nsp, n1, n2)),
        out_shape=jax.ShapeDtypeStruct((rows // 2, total_cols), BF16),
        in_specs=[hbm, vmem, hbm, hbm, hbm, hbm] + [vmem] * 10 + [hbm, hbm],
        out_specs=vmem,
        scratch_shapes=[
            pltpu.VMEM((2, rows, half), BF16),
            pltpu.VMEM(in_gain.shape, BF16),
            pltpu.VMEM((4, 2, half, inner), BF16),
            pltpu.VMEM(w_out_ssm.shape, BF16),
            pltpu.VMEM(w_out_conv.shape, BF16),
            pltpu.VMEM((2, rows, half), BF16),
            pltpu.VMEM((blocks, 128, 2 * wide), BF16),
            pltpu.VMEM((blocks, 128, 2 * wide), BF16),
            pltpu.VMEM((rows * lines, 128), F32),
            pltpu.VMEM((rows * lines, 128), F32),
            pltpu.VMEM((rows * lines, 128), F32),
            pltpu.VMEM((rows + 8, w_bgate.shape[1]), F32),
            pltpu.VMEM((8, w_bgate.shape[1]), F32),
            pltpu.VMEM((rows, total_cols), F32),
            pltpu.VMEM((rows, inner), BF16),
            pltpu.VMEM((3, lines, 128), F32),
            pltpu.VMEM((n1, 3, lines, 128), F32),
            pltpu.VMEM((3, lines, 128), F32),
            pltpu.VMEM((n2, 3, lines, 128), F32),
            pltpu.VMEM((chunks, rows, total_cols // chunks), BF16),
            pltpu.VMEM((chunks, rows // 2, total_cols // chunks), BF16),
            dma((11,)),
            dma((2,)),
            dma((2,)),
            dma((n1,)),
            dma((n1,)),
            dma((n2,)),
            dma((n2,)),
            dma((1,)),
            dma((1,)),
            dma((chunks,)),
            dma((chunks,)),
        ],
        compiler_params=pltpu.CompilerParams(
            collective_id=0, has_side_effects=True, vmem_limit_bytes=56 * 1024 * 1024
        ),
    )(
        tokens, in_gain, w_input, w_bgate, w_cgate, w_value, decay_rate, angle, decay_shift,
        b_input.transpose(0, 1, 3, 2), c_output, init,
        skip_gain.reshape(1, -1), ssm_gain.reshape(1, -1), conv_gain.reshape(1, -1),
        conv_taps, w_out_ssm, w_out_conv,
    )


def solution(mesh):
    return jax.shard_map(
        functools.partial(body, mesh.shape["sp"]),
        mesh=mesh,
        in_specs=(
            P("sp", "tp"),
            P(None, "tp"),
            P(None, "tp"),
            P(None, "tp"),
            P(None, "tp"),
            P(None, "tp"),
            P("tp", None),
            P("tp", None),
            P("tp", "sp"),
            P(None, "tp", None, None),
            P(None, "tp", None, None),
            P(None, "tp", None),
            P("tp"),
            P("tp"),
            P("tp"),
            P(None, "tp"),
            P("tp", None),
            P("tp", None),
        ),
        out_specs=P(("sp", "tp"), None),
        check_vma=False,
    )
```

time: 264 us -> 23.7 us (0.09)
  blocking collectives: 167 us -> 0 us
  matrix products: 33.2 us -> 0 us
  Pallas kernels: 0 us -> 21.9 us
  other arithmetic: 18.4 us -> 0 us
  local copies, waits for them, and re-layouts: 17.9 us -> 1.67 us
  between operations: 13.8 us -> 0.01 us
  waiting for transfers between devices: 5.66 us -> 0 us
  starting transfers between devices: 4.73 us -> 0 us
    all_gather x6 -> x0, blocking collectives: 167 us -> none  [the longest x4 163 us: entering(): pieces = jax.tree.map(lambda part: lax.all_gather(part, axis), value)]
    dot_general x10 -> x0, matrix products: 33.2 us -> none  [the longest x1 10.2 us: local_chain(): summed_re = jnp.dot(lower, quot_re, precision=highest)]
    pallas_call x0 -> x1, Pallas kernels: none -> 21.9 us  [body(): pl.pallas_call(functools.partial(kernel, (nsp, n1, n2)), out_shape=jax.Sh...]
    select_n x15 -> x0, other arithmetic: 11.9 us -> none  [hop(): jnp.where(position < mine, new, old)]
    reshape x4 -> x0, local copies, waits for them, and re-layouts: 7.76 us -> none  [the longest x1 2.58 us: local_chain(): log_mag = jnp.repeat(local_log, entries, axis=1) - counted * rate_flat]
    reduce_scatter x1 -> x0, waiting for transfers between devices: 5.64 us -> none  [body(): lax.psum_scatter((result + jnp.dot(conv_out, w_out_conv, preferred_elemen...]
    ppermute x1 -> x0, starting transfers between devices: 4.73 us -> none  [from_behind(): lax.ppermute(value, axis, [(source, source + steps) for source in range(i...]
    add x2 -> x0, other arithmetic: 3.67 us -> none  [the longest x1 3.66 us: body(): cum[3] + cum[0] * entry_im + cum[1] * entry_re]
  transfers between devices with their start and end apart: 2 -> 0, of which waited for: 1 -> 0; matrix products, arithmetic and copies ran while one was open for 22% -> 0% of each run, Pallas kernels for 0% -> 0%
where the time goes in v1:
time: 23.7 us; the launch traced here: 23.6 us
  Pallas kernels  21.9 us (92%)
  local copies, waits for them, and re-layouts  1.67 us (7%)
    pallas_call x1, Pallas kernels, body(): pl.pallas_call(functools.partial(kernel, (nsp, n1, n2)), out_shape=jax.Sh...  21.9 us
    unnamed x1, local copies, waits for them, and re-layouts  1.67 us

profile of v1, /device:TPU:0, one launch (start us, length us, event | category | flops | bytes accessed | tf_op | source)
XLA Modules:
  0.0 23.6 jit_solution(3879642865410577144)
XLA Ops:
  0.0 21.9 %shard_map.172 = bf16[64,2048]{1,0:T(8,128)(2,1)} custom-call(bf16[128,1024]{1,0:T(8,128)(2,1)} %tok_h.1, bf16[1,1024]{1,0:T(2,128)(2,1)} %gain.1, bf16[2048,512]{1,0:T(8,128)(2,1)} %w_in_h.1, bf16[2048,512]{1,0:T(8,128)(2,1)} %w_bg_h.1, bf16[2048,512]{1,0:T(8,128)(2,1)} %w_cg_h.1, bf16[2048,512]{1,0:T(8,128)(2,1)} %w_va_h.1, f32[32,64]{1,0:T(8,128)} %rate.1, ...), custom_call_target="tpu_custom_call" | custom-call | tf_op jit(solution)/shard_map/pallas_call | solution.py:352
  21.9 1.7 %copy.20 = bf16[64,2048]{1,0:T(8,128)(2,1)} copy(bf16[64,2048]{1,0:T(8,128)(2,1)} %shard_map.172) | data formatting | bytes 524288

commit v2 on v1

--- a/solution.py
+++ b/solution.py
@@ -52,19 +52,19 @@
 
 def kernel(
     sizes,
-    tok_h, gain, w_in_h, w_bg_h, w_cg_h, w_va_h, rate, angle, shift, b_in, c_out, init,
+    tok_h, gain, w_in_h, w_bg_h, w_cg_h, w_va_h, rate, angle, shift, b_h, c_h, init,
     skip, sgain, cgain, taps, wos_h, woc_h,
-    out,
-    tok, gain_o, w, wos, woc, sc, bx, cx, e_s, d_re, d_im, gated, halo, acc, ssm_b,
-    mine1, slots1, mine2, slots2, part_s, part_r,
+    out_own, out_oth,
+    tok, b_in, c_out, gain_o, w, wos, woc, sc, bx, cx, e_s, d_re, d_im, gated, halo, acc, ssm_b,
+    mine1, slots1, mine2, slots2, part_s,
     loc_sem, tok_send, tok_recv, ph1_send, ph1_recv, ph2_send, ph2_recv, halo_send, halo_recv,
-    out_send, out_recv,
+    out_send, out_recv, own_sem,
 ):
     nsp, n1, n2 = sizes
     sp, tp = lax.axis_index("sp"), lax.axis_index("tp")
     rows, half = tok_h.shape
     groups, entries = rate.shape
-    ch = c_out.shape[2]
+    ch = c_h.shape[2]
     per = 128 // ch
     width = groups * entries
     lines = width // 128
@@ -87,8 +87,10 @@
             )
     copies.append(pltpu.make_async_copy(woc_h, woc, loc_sem.at[len(copies)]))
     copies.append(pltpu.make_async_copy(wos_h, wos, loc_sem.at[len(copies)]))
-    for copy in copies:
-        copy.start()
+    copies.append(pltpu.make_async_copy(b_h, b_in, loc_sem.at[len(copies)]))
+    copies.append(pltpu.make_async_copy(c_h, c_out, loc_sem.at[len(copies)]))
+    for k in (0, 1, 11, 2, 12, 3, 4):
+        copies[k].start()
 
     peers1 = [outer * n1 + lax.rem(inner + k, n1) for k in range(1, n1)]
     peers2 = [lax.rem(outer + k, n2) * n1 + inner for k in range(1, n2)]
@@ -96,7 +98,6 @@
     pl.semaphore_signal(barrier, inc=1, device_id={"tp": 1 - tp}, device_id_type=MESH)
     for peer in peers1 + peers2 + [nxt, prv]:
         pl.semaphore_signal(barrier, inc=1, device_id={"sp": peer}, device_id_type=MESH)
-    pl.semaphore_wait(barrier, 1 + len(peers1) + len(peers2) + 2)
 
     def remote(src, dst, send, recv, **where):
         return pltpu.make_async_remote_copy(
@@ -104,24 +105,12 @@
             device_id=where, device_id_type=MESH,
         )
 
-    swap_tok = remote(tok_h, tok.at[1], tok_send.at[0], tok_recv.at[0], tp=1 - tp)
+    swap_tok = remote(tok.at[0], tok.at[1], tok_send.at[0], tok_recv.at[0], tp=1 - tp)
     swap_gain = remote(gain, gain_o, tok_send.at[1], tok_recv.at[1], tp=1 - tp)
-    swap_tok.start()
-    swap_gain.start()
-
-    bx[...] = jnp.zeros_like(bx)
-    cx[...] = jnp.zeros_like(cx)
-    zr, zi = zoh_of(rate[...], angle[...])
-    for g in range(groups):
-        q, k = g // per, g % per
-        r, l = k * ch, k * entries
-        gr, gi = zr[g : g + 1, :], zi[g : g + 1, :]
-        b0, b1 = b_in[0, g], b_in[1, g]
-        bx[q, r : r + ch, l : l + entries] = (gr * b0 - gi * b1).astype(BF16)
-        bx[q, r : r + ch, wide + l : wide + l + entries] = (gr * b1 + gi * b0).astype(BF16)
-        cx[q, r : r + ch, l : l + entries] = c_out[0, g].astype(BF16)
-        cx[q, r : r + ch, wide + l : wide + l + entries] = (-c_out[1, g]).astype(BF16)
-
+    copies[0].wait()
+    floats = tok[0].astype(F32)
+    sc[0] = (floats * gain[...].astype(F32)).astype(BF16)
+    squares = jnp.sum(floats * floats, axis=1, keepdims=True)
     parts = jnp.concatenate(split3(jnp.exp(shift[...])), axis=0)
     count = parts.shape[0]
     pad = -count % 128
@@ -144,12 +133,29 @@
     size = jnp.exp(-rate_p)
     lam_re, lam_im = size * jnp.cos(angle_p), size * jnp.sin(angle_p)
 
-    copies[0].wait()
-    floats = tok[0].astype(F32)
-    sc[0] = (floats * gain[...].astype(F32)).astype(BF16)
-    squares = jnp.sum(floats * floats, axis=1, keepdims=True)
+    pl.semaphore_wait(barrier, 1 + len(peers1) + len(peers2) + 2)
+    swap_tok.start()
+    swap_gain.start()
+
+    bx[...] = jnp.zeros_like(bx)
+    cx[...] = jnp.zeros_like(cx)
+    copies[11].wait()
+    copies[12].wait()
+    zr, zi = zoh_of(rate[...], angle[...])
+    for g in range(groups):
+        q, k = g // per, g % per
+        r, l = k * ch, k * entries
+        gr, gi = zr[g : g + 1, :], zi[g : g + 1, :]
+        b0, b1 = b_in[0, g], b_in[1, g]
+        bx[q, r : r + ch, l : l + entries] = (gr * b0 - gi * b1).astype(BF16)
+        bx[q, r : r + ch, wide + l : wide + l + entries] = (gr * b1 + gi * b0).astype(BF16)
+        cx[q, r : r + ch, l : l + entries] = c_out[0, g].astype(BF16)
+        cx[q, r : r + ch, wide + l : wide + l + entries] = (-c_out[1, g]).astype(BF16)
+
     copies[1].wait()
     total = dot(sc[0], w[0, 0])
+    for k in range(5, 11):
+        copies[k].start()
     swap_tok.wait()
     swap_gain.wait()
     floats = tok[1].astype(F32)
@@ -174,7 +180,7 @@
         new_im = (a_re * s_im + a_im * s_re) + d_im[here, :]
         return here, decay, new_re, new_im
 
-    unroll = 8
+    unroll = 32
     nil = jnp.zeros((lines, 128), F32)
 
     def first_pass(t, carry):
@@ -311,23 +317,31 @@
 
     copies[10].wait()
     total_cols = wos.shape[1]
-    chunks = part_r.shape[0]
+    chunks = part_s.shape[0]
     step = total_cols // chunks
     part_rows = rows // 2
     own = pl.ds(pl.multiple_of(tp * part_rows, part_rows), part_rows)
     other = pl.ds(pl.multiple_of((1 - tp) * part_rows, part_rows), part_rows)
-    sends = []
+    sends, keeps = [], []
     for c in range(chunks):
         cols = slice(c * step, (c + 1) * step)
         part_s[c] = (acc[:, cols] + dot(ssm_b[...], wos[:, cols])).astype(BF16)
         sends.append(
-            remote(part_s.at[c, other], part_r.at[c], out_send.at[c], out_recv.at[c], tp=1 - tp)
+            remote(
+                part_s.at[c, other], out_oth.at[:, pl.ds(c * step, step)],
+                out_send.at[c], out_recv.at[c], tp=1 - tp,
+            )
         )
         sends[-1].start()
+        keeps.append(
+            pltpu.make_async_copy(
+                part_s.at[c, own], out_own.at[:, pl.ds(c * step, step)], own_sem.at[c]
+            )
+        )
+        keeps[-1].start()
     for c in range(chunks):
+        keeps[c].wait()
         sends[c].wait()
-        cols = slice(c * step, (c + 1) * step)
-        out[:, cols] = (part_s[c, own].astype(F32) + part_r[c].astype(F32)).astype(BF16)
 
 
 def body(
@@ -349,13 +363,16 @@
     vmem = pl.BlockSpec(memory_space=pltpu.VMEM)
     hbm = pl.BlockSpec(memory_space=pl.ANY)
     dma = pltpu.SemaphoreType.DMA
-    return pl.pallas_call(
+    result = jax.ShapeDtypeStruct((rows // 2, total_cols), BF16)
+    own, other = pl.pallas_call(
         functools.partial(kernel, (nsp, n1, n2)),
-        out_shape=jax.ShapeDtypeStruct((rows // 2, total_cols), BF16),
-        in_specs=[hbm, vmem, hbm, hbm, hbm, hbm] + [vmem] * 10 + [hbm, hbm],
-        out_specs=vmem,
+        out_shape=(result, result),
+        in_specs=[hbm, vmem, hbm, hbm, hbm, hbm] + [vmem] * 3 + [hbm, hbm] + [vmem] * 5 + [hbm, hbm],
+        out_specs=(hbm, hbm),
         scratch_shapes=[
             pltpu.VMEM((2, rows, half), BF16),
+            pltpu.VMEM((2, groups, ch, entries), F32),
+            pltpu.VMEM(c_output.shape, F32),
             pltpu.VMEM(in_gain.shape, BF16),
             pltpu.VMEM((4, 2, half, inner), BF16),
             pltpu.VMEM(w_out_ssm.shape, BF16),
@@ -375,8 +392,7 @@
             pltpu.VMEM((3, lines, 128), F32),
             pltpu.VMEM((n2, 3, lines, 128), F32),
             pltpu.VMEM((chunks, rows, total_cols // chunks), BF16),
-            pltpu.VMEM((chunks, rows // 2, total_cols // chunks), BF16),
-            dma((11,)),
+            dma((13,)),
             dma((2,)),
             dma((2,)),
             dma((n1,)),
@@ -385,6 +401,7 @@
             dma((n2,)),
             dma((1,)),
             dma((1,)),
+            dma((chunks,)),
             dma((chunks,)),
             dma((chunks,)),
         ],
@@ -397,6 +414,7 @@
         skip_gain.reshape(1, -1), ssm_gain.reshape(1, -1), conv_gain.reshape(1, -1),
         conv_taps, w_out_ssm, w_out_conv,
     )
+    return (own.astype(F32) + other.astype(F32)).astype(BF16)
 
 
 def solution(mesh):

time: 23.7 us -> 23.1 us (0.975)
  other arithmetic: 0 us -> 1.8 us
  local copies, waits for them, and re-layouts: 1.67 us -> 0 us
  Pallas kernels: 21.9 us -> 21.1 us
    convert_element_type x0 -> x1, other arithmetic: none -> 1.8 us  [body(): return (own.astype(F32) + other.astype(F32)).astype(BF16)]
    unnamed x1 -> x0, local copies, waits for them, and re-layouts: 1.67 us -> none
    pallas_call x1, Pallas kernels: 21.9 us -> 21.1 us  [body(): pl.pallas_call(functools.partial(kernel, (nsp, n1, n2)), out_shape=(resul...]
where the time goes in v2:
time: 23.1 us; the launch traced here: 22.9 us
  Pallas kernels  21.1 us (91%)
  other arithmetic  1.8 us (8%)
    pallas_call x1, Pallas kernels, body(): pl.pallas_call(functools.partial(kernel, (nsp, n1, n2)), out_shape=(resul...  21.1 us
    convert_element_type x1, other arithmetic, body(): return (own.astype(F32) + other.astype(F32)).astype(BF16)  1.8 us

profile of v2, /device:TPU:0, one launch (start us, length us, event | category | flops | bytes accessed | tf_op | source)
XLA Modules:
  0.0 22.9 jit_solution(3036052749109154248)
XLA Ops:
  0.0 21.1 %shard_map.172 = (bf16[64,2048]{1,0:T(8,128)(2,1)}, bf16[64,2048]{1,0:T(8,128)(2,1)}) custom-call(bf16[128,1024]{1,0:T(8,128)(2,1)} %tok_h.1, bf16[1,1024]{1,0:T(2,128)(2,1)} %gain.1, bf16[2048,512]{1,0:T(8,128)(2,1)} %w_in_h.1, bf16[2048,512]{1,0:T(8,128)(2,1)} %w_bg_h.1, bf16[2048,512]{1,0:T(8,128)(2,1)} %w_cg_h.1, bf16[2048,512]{1,0:T(8,128)(2,1)} %w_va_h.1, ...), custom_call_target="tpu_custom_call" | custom-call | tf_op jit(solution)/shard_map/pallas_call | solution.py:367
  21.1 1.8 %add_convert_fusion = bf16[64,2048]{1,0:T(8,128)(2,1)} fusion(bf16[64,2048]{1,0:T(8,128)(2,1)} %get-tuple-element.8, bf16[64,2048]{1,0:T(8,128)(2,1)} %get-tuple-element.7), kind=kLoop, calls=%fused_computation | loop fusion | flops 524288 | bytes 786432 | tf_op jit(solution)/shard_map/convert_element_type | solution.py:417
